TPU v7x, 128 devices: a whole 4x4x4 slice. The times are simulated.
128 devices in a mesh: sp: 32 (over z, y, core), tp: 4 (over x).
Axes of the slice: x: 4, y: 4, z: 4, core: 2. Of those that a mesh axis runs over, the one named last changes fastest.
Arguments:
- residual_entry_input: bfloat16 [32768, 2048], P(('sp', 'tp')), may hold values from -6 to 6
- query_matrix_rows: bfloat16 [32768, 1024], P('sp', 'tp'), may hold values from -6 to 6
- key_matrix_rows: bfloat16 [32768, 1024], P('sp', 'tp'), may hold values from -6 to 6
- value_matrix_rows: bfloat16 [32768, 2048], P('sp', 'tp'), may hold values from -6 to 6
- output_gate_logits: bfloat16 [32768, 2048], P('sp', 'tp'), may hold values from -6 to 6
- input_gate_logits: float32 [32768, 8], P('sp', 'tp'), may hold values from -6 to 6
- forget_gate_logits: float32 [32768, 8], P('sp', 'tp'), may hold values from -8 to 31
- forget_decay_offset: float32 [32768, 8], P('sp', 'tp'), may hold values from -0.7 to 0
- head_norm_gain: float32 [8, 256], P('tp'), may hold values from 0.1 to 1.9
- cell_output_weight: bfloat16 [2048, 2048], P('tp'), may hold values from -0.125 to 0.125
- feedforward_norm_gain: float32 [2048], replicated, may hold values from 0.1 to 1.9
- gate_up_weight: bfloat16 [2048, 5632], P('sp', 'tp'), may hold values from -0.125 to 0.125
- value_up_weight: bfloat16 [2048, 5632], P('sp', 'tp'), may hold values from -0.125 to 0.125
- gate_filter_taps: float32 [3, 5632], P(None, 'tp'), may hold values from -3 to 3
- value_filter_taps: float32 [3, 5632], P(None, 'tp'), may hold values from -3 to 3
- down_projection_weight: bfloat16 [5632, 2048], P('tp', 'sp'), may hold values from -0.078125 to 0.078125
Outputs:
- result: bfloat16 [32768, 2048], P(('sp', 'tp'))
All inputs are finite; a program needn't handle non-finite values.
Results may differ from a plain program's by a relative error of at most 0.025.
Values may be sent and summed in bfloat16 or wider, within the bound.
A program may use at most 128 MiB of HBM per device.

v0:
```python
import jax
import jax.numpy as jnp
from jax import lax
from jax.sharding import Mesh
from jax.sharding import PartitionSpec as P

BLOCK = 128
SP = ("sp_0", "sp_1", "sp_2")
SP_TP = ("sp_0", "sp_1", "sp_2", "tp")
eps = 1e-06
neg_large = -1e30


def neutral_like(x, identity):
    return jax.tree.map(
        lambda part, zero: jnp.zeros_like(part) + jnp.asarray(zero, part.dtype), x, identity
    )


def gathered_once(x, axis):
    leaves = jax.tree.leaves(x)
    sequence = sorted(range(len(leaves)), key=lambda k: -leaves[k].size)
    width = (1, *leaves[sequence[0]].shape)[-1]
    lines = [
        jnp.pad(leaves[k].reshape(-1), (0, -leaves[k].size % width)).reshape(-1, width)
        for k in sequence
    ]
    both, at, found = (lax.all_gather(jnp.concatenate(lines), axis), 0, {})
    for k, line in zip(sequence, lines):
        slab = both[:, at : at + len(line)].reshape(len(both), -1)
        found[k] = slab[:, : leaves[k].size].reshape(-1, *leaves[k].shape)
        at += len(line)
    numbers = iter(range(len(leaves)))
    return jax.tree.map(lambda _: found[next(numbers)], x)


def entering(x, axes, combine, identity):
    before = start = neutral_like(x, identity)
    running = x
    for axis in reversed(axes):
        count, position = (lax.axis_size(axis), lax.axis_index(axis))
        pieces = gathered_once(
            jax.tree.map(
                lambda part, kind: part.astype(kind),
                running,
                (jnp.bfloat16, jnp.bfloat16, jnp.bfloat16, jnp.bfloat16),
            ),
            axis,
        )
        inside, running = (start, start)
        for k in range(count):
            passed = k < position
            running = combine(
                running, jax.tree.map(lambda part, own: part[k].astype(own.dtype), pieces, x)
            )
            inside = jax.tree.map(lambda new, old: jnp.where(passed, new, old), running, inside)
        before = combine(inside, before)
    return before


def shifted(x, axis, by):
    count = lax.axis_size(axis)
    pairs = [(i, i + by) for i in range(count) if 0 <= i + by < count]
    return lax.ppermute(x, axis, pairs)


def side_by_side(arrays, axis, dim, along):
    both = jnp.concatenate(arrays, axis=along)
    result, at, finished = (lax.all_gather(both, axis, axis=dim, tiled=True), 0, [])
    for a in arrays:
        finished.append(lax.slice_in_dim(result, at, at + a.shape[along], axis=along))
        at += a.shape[along]
    return tuple(finished)


def laid_out(tiles, dim):
    shape = list(tiles.shape[1:])
    shape[dim] *= tiles.shape[0]
    return jnp.moveaxis(tiles, 0, dim).reshape(shape)


def all_blocks(x, axes, sequence):
    tiles = x
    for k in sequence:
        tiles = lax.all_gather(tiles, axes[k])
    done = sequence[::-1]
    back = [done.index(k) for k in range(len(axes))]
    tiles = tiles.transpose(*back, *range(len(axes), tiles.ndim))
    return tiles.reshape(-1, *x.shape)


def gather_axes(x, axes, sequence, dim):
    return laid_out(all_blocks(x, axes, sequence), dim)


def gate_log_values(input_gate_logits, forget_gate_logits, forget_decay_offset):
    input_log_value = 15.0 * jnp.tanh(input_gate_logits / 15.0)
    forget_log_sigmoid = (
        jax.nn.log_sigmoid(15.0 * jnp.tanh(forget_gate_logits / 15.0)) + forget_decay_offset
    )
    return (input_log_value, forget_log_sigmoid)


def combine_states(earlier, later):
    total_one, memory_one, normer_one, running_one = earlier
    total_two, memory_two, normer_two, running_two = later
    joined = jnp.maximum(total_two + running_one, running_two)
    weight_one = jnp.exp(total_two + running_one - joined)
    weight_two = jnp.exp(running_two - joined)
    memory = weight_one[:, None, None] * memory_one + weight_two[:, None, None] * memory_two
    normer = weight_one[:, None] * normer_one + weight_two[:, None] * normer_two
    return (total_one + total_two, memory, normer, joined)


def local_step(state_carry, inputs):
    memory, normer, running = state_carry
    query_block, key_block, value_block, input_block, forget_block = inputs
    length = query_block.shape[0]
    highest = lax.Precision.DEFAULT
    query_scale = query_block.shape[2] ** (-0.5)
    causal = jnp.tril(jnp.ones((length, length), dtype=bool))[:, :, None]
    cumulative = jnp.cumsum(forget_block, axis=0)
    logits = cumulative[:, None, :] - cumulative[None, :, :] + input_block[None, :, :]
    logits = jnp.where(causal, logits, -jnp.inf)
    carried = cumulative + running[None, :]
    stable = jnp.maximum(carried, jnp.max(logits, axis=1))
    carry_weight = jnp.exp(carried - stable)
    raw = (
        jnp.einsum("thd,shd->tsh", query_block, key_block, preferred_element_type=jnp.float32)
        * query_scale
    )
    scores = raw * jnp.exp(logits - stable[:, None, :])
    scaled_query = query_block.astype(jnp.float32) * query_scale
    numerator = carry_weight[:, :, None] * jnp.einsum(
        "hvd,thd->thv", memory, scaled_query, precision=highest
    )
    numerator = numerator + jnp.einsum(
        "tsh,shv->thv", scores.astype(jnp.bfloat16), value_block, preferred_element_type=jnp.float32
    )
    denominator = carry_weight * jnp.einsum(
        "hd,thd->th", normer, scaled_query, precision=highest
    ) + jnp.sum(scores, axis=1)
    last_sum = cumulative[-1]
    weights_log = last_sum[None, :] - cumulative + input_block
    new_running = jnp.maximum(last_sum + running, jnp.max(weights_log, axis=0))
    decay_factor = jnp.exp(last_sum + running - new_running)
    weighted = (
        key_block.astype(jnp.float32) * jnp.exp(weights_log - new_running[None, :])[:, :, None]
    )
    memory = decay_factor[:, None, None] * memory + jnp.einsum(
        "shv,shd->hvd",
        value_block,
        weighted.astype(jnp.bfloat16),
        preferred_element_type=jnp.float32,
    )
    normer = decay_factor[:, None] * normer + jnp.sum(weighted, axis=0)
    return ((memory, normer, new_running), (numerator, denominator, stable))


def local(
    residual_entry_input,
    query_matrix_rows,
    key_matrix_rows,
    value_matrix_rows,
    output_gate_logits,
    input_gate_logits,
    forget_gate_logits,
    forget_decay_offset,
    head_norm_gain,
    cell_output_weight,
    feedforward_norm_gain,
    gate_up_weight,
    value_up_weight,
    gate_filter_taps,
    value_filter_taps,
    down_projection_weight,
):
    highest = lax.Precision.DEFAULT
    token_count = query_matrix_rows.shape[0]
    head_count = input_gate_logits.shape[1]
    key_width = query_matrix_rows.shape[1] // head_count
    value_width = value_matrix_rows.shape[1] // head_count
    query_scale = key_width ** (-0.5)
    queries_low = query_matrix_rows.reshape(token_count, head_count, key_width)
    keys_low = key_matrix_rows.reshape(token_count, head_count, key_width)
    values_low = value_matrix_rows.reshape(token_count, head_count, value_width)
    input_log_value, forget_log_sigmoid = gate_log_values(
        input_gate_logits, forget_gate_logits, forget_decay_offset
    )
    cumulative = jnp.cumsum(forget_log_sigmoid, axis=0)
    total_log = cumulative[-1]
    block_count = token_count // BLOCK

    def blocks(tensor):
        return tensor.reshape((block_count, BLOCK) + tensor.shape[1:])

    initial = (
        jnp.zeros((head_count, value_width, key_width), jnp.float32),
        jnp.zeros((head_count, key_width), jnp.float32),
        jnp.full((head_count,), neg_large, jnp.float32),
    )
    end_state, (numerator, denominator, stable) = lax.scan(
        local_step,
        initial,
        (
            blocks(queries_low),
            blocks(keys_low),
            blocks(values_low),
            blocks(input_log_value),
            blocks(forget_log_sigmoid),
        ),
    )
    end_memory, end_normer, end_running = end_state
    identity = (
        jnp.zeros((head_count,), jnp.float32),
        jnp.zeros((head_count, value_width, key_width), jnp.float32),
        jnp.zeros((head_count, key_width), jnp.float32),
        jnp.full((head_count,), neg_large, jnp.float32),
    )
    prefix = entering(
        (total_log, end_memory, end_normer, end_running), SP, combine_states, identity
    )
    numerator = numerator.reshape(token_count, head_count, value_width)
    denominator = denominator.reshape(token_count, head_count)
    stable = stable.reshape(token_count, head_count)
    _, prior_memory, prior_normer, prior_running = prefix
    scaled_query = queries_low.astype(jnp.float32) * query_scale
    prior_log = cumulative + prior_running[None, :]
    top_log = jnp.maximum(stable, prior_log)
    local_weight = jnp.exp(stable - top_log)
    prior_weight = jnp.exp(prior_log - top_log)
    numerator = local_weight[:, :, None] * numerator + prior_weight[:, :, None] * jnp.einsum(
        "hvd,thd->thv", prior_memory, scaled_query, precision=highest
    )
    denominator = local_weight * denominator + prior_weight * jnp.einsum(
        "hd,thd->th", prior_normer, scaled_query, precision=highest
    )
    memory_out = numerator / jnp.maximum(jnp.abs(denominator), jnp.exp(-top_log))[:, :, None]
    normed = (
        memory_out
        * lax.rsqrt(jnp.mean(memory_out * memory_out, axis=-1, keepdims=True) + eps)
        * head_norm_gain[None, :, :]
    )
    gated_rows = (
        normed.reshape(token_count, head_count * value_width)
        * jax.nn.sigmoid(output_gate_logits.astype(jnp.float32))
    ).astype(jnp.bfloat16)
    whole_out = lax.all_gather(cell_output_weight, "tp", axis=0, tiled=True)
    own_rows = lax.all_to_all(gated_rows, "tp", split_axis=0, concat_axis=1, tiled=True)
    mixed_rows = jnp.dot(own_rows, whole_out, preferred_element_type=jnp.float32)
    stream_wide = residual_entry_input.astype(jnp.float32) + mixed_rows
    stream = stream_wide.astype(jnp.bfloat16)
    stream_wide = lax.optimization_barrier(stream).astype(jnp.float32)
    normed_rows = (
        stream_wide
        * lax.rsqrt(jnp.mean(stream_wide * stream_wide, axis=-1, keepdims=True) + eps)
        * feedforward_norm_gain[None, :]
    ).astype(jnp.bfloat16)
    group_rows = lax.all_gather(normed_rows, "tp", axis=0, tiled=True)
    earlier_rows = shifted(group_rows[-2:], SP, 1)
    window = jnp.concatenate([earlier_rows, group_rows], axis=0)
    pieces = side_by_side((gate_up_weight, value_up_weight), SP, 0, 1)
    up_gate = jnp.dot(window, pieces[0], preferred_element_type=jnp.float32)
    up_value = jnp.dot(window, pieces[1], preferred_element_type=jnp.float32)
    conv_g = (
        gate_filter_taps[0][None, :] * up_gate[:-2]
        + gate_filter_taps[1][None, :] * up_gate[1:-1]
        + gate_filter_taps[2][None, :] * up_gate[2:]
    )
    conv_v = (
        value_filter_taps[0][None, :] * up_value[:-2]
        + value_filter_taps[1][None, :] * up_value[1:-1]
        + value_filter_taps[2][None, :] * up_value[2:]
    )
    hidden = (jax.nn.silu(conv_g) * conv_v).astype(jnp.bfloat16)
    whole_down = gather_axes(down_projection_weight, (("sp_0", "sp_1"), "sp_2"), (0, 1), 1)
    ffn_rows = lax.psum_scatter(
        jnp.dot(hidden, whole_down, preferred_element_type=jnp.float32).astype(jnp.bfloat16),
        "tp",
        scatter_dimension=0,
        tiled=True,
    ).astype(jnp.float32)
    return (stream_wide + ffn_rows).astype(jnp.bfloat16)


def solution(mesh):
    split = Mesh(mesh.devices.reshape(4, 4, 2, mesh.shape["tp"]), ("sp_0", "sp_1", "sp_2", "tp"))
    placed = (
        P(SP_TP, None),
        P(SP, "tp"),
        P(SP, "tp"),
        P(SP, "tp"),
        P(SP, "tp"),
        P(SP, "tp"),
        P(SP, "tp"),
        P(SP, "tp"),
        P("tp", None),
        P("tp", None),
        P(),
        P(SP, "tp"),
        P(SP, "tp"),
        P(None, "tp"),
        P(None, "tp"),
        P("tp", SP),
    )
    return jax.shard_map(
        local, mesh=split, in_specs=placed, out_specs=P(SP_TP, None), check_vma=False
    )
```

profile of v0, /device:TPU:1, one launch (start us, length us, event | category | flops | bytes accessed | tf_op | source)
XLA Modules:
  0.0 419.1 jit_solution(10256180526580571442)
XLA Ops:
  13.6 102.5 %while.21 = (s32[]{:T(128)}, f32[2,256,128]{2,1,0:T(8,128)S(1)}, f32[2,128]{1,0:T(2,128)S(1)}, f32[2]{0:T(128)S(1)}, f32[8,128,2,256]{1,0,3,2:T(8,128)}, /*index...) while((s32[]{:T(128)}, f32[2,256,128]{2,1,0:T(8,128)S(1)}, ...), condition=%wide.region_6.7_spmd.clone, body=%wide.region_0.6_spmd.clone.sunk | while | flops 59952648 | bytes 4685610 | solution.py:202
  17.8 8.3 %dynamic_update_slice.19 = f32[8,128,2,256]{1,0,3,2:T(8,128)} dynamic-update-slice(f32[8,128,2,256]{1,0,3,2:T(8,128)} %get-tuple-element.428, f32[1,128,2,256]{1,0,3,2:T(1,128)S(1)} %copy.336, s32[]{:T(128)} %get-tuple-element.424, s32[]{:T(128)} %constant.38.clone.1..sunk, s32[]{:T(128)} %constant.38.clone.1..sunk, s32[]{:T(128)} %constant.38.clone.1..sunk) | dynamic-update-slice | bytes 524292 | tf_op jit(solution)/shard_map/while/body/jit(dynamic_update_index_in_dim)/dynamic_update_slice | solution.py:202
  30.7 8.2 %dynamic_update_slice.19 = f32[8,128,2,256]{1,0,3,2:T(8,128)} dynamic-update-slice(f32[8,128,2,256]{1,0,3,2:T(8,128)} %get-tuple-element.428, f32[1,128,2,256]{1,0,3,2:T(1,128)S(1)} %copy.336, s32[]{:T(128)} %get-tuple-element.424, s32[]{:T(128)} %constant.38.clone.1..sunk, s32[]{:T(128)} %constant.38.clone.1..sunk, s32[]{:T(128)} %constant.38.clone.1..sunk) | dynamic-update-slice | bytes 524292 | tf_op jit(solution)/shard_map/while/body/jit(dynamic_update_index_in_dim)/dynamic_update_slice | solution.py:202
  43.5 8.2 %dynamic_update_slice.19 = f32[8,128,2,256]{1,0,3,2:T(8,128)} dynamic-update-slice(f32[8,128,2,256]{1,0,3,2:T(8,128)} %get-tuple-element.428, f32[1,128,2,256]{1,0,3,2:T(1,128)S(1)} %copy.336, s32[]{:T(128)} %get-tuple-element.424, s32[]{:T(128)} %constant.38.clone.1..sunk, s32[]{:T(128)} %constant.38.clone.1..sunk, s32[]{:T(128)} %constant.38.clone.1..sunk) | dynamic-update-slice | bytes 524292 | tf_op jit(solution)/shard_map/while/body/jit(dynamic_update_index_in_dim)/dynamic_update_slice | solution.py:202
  56.3 8.2 %dynamic_update_slice.19 = f32[8,128,2,256]{1,0,3,2:T(8,128)} dynamic-update-slice(f32[8,128,2,256]{1,0,3,2:T(8,128)} %get-tuple-element.428, f32[1,128,2,256]{1,0,3,2:T(1,128)S(1)} %copy.336, s32[]{:T(128)} %get-tuple-element.424, s32[]{:T(128)} %constant.38.clone.1..sunk, s32[]{:T(128)} %constant.38.clone.1..sunk, s32[]{:T(128)} %constant.38.clone.1..sunk) | dynamic-update-slice | bytes 524292 | tf_op jit(solution)/shard_map/while/body/jit(dynamic_update_index_in_dim)/dynamic_update_slice | solution.py:202
  69.1 8.2 %dynamic_update_slice.19 = f32[8,128,2,256]{1,0,3,2:T(8,128)} dynamic-update-slice(f32[8,128,2,256]{1,0,3,2:T(8,128)} %get-tuple-element.428, f32[1,128,2,256]{1,0,3,2:T(1,128)S(1)} %copy.336, s32[]{:T(128)} %get-tuple-element.424, s32[]{:T(128)} %constant.38.clone.1..sunk, s32[]{:T(128)} %constant.38.clone.1..sunk, s32[]{:T(128)} %constant.38.clone.1..sunk) | dynamic-update-slice | bytes 524292 | tf_op jit(solution)/shard_map/while/body/jit(dynamic_update_index_in_dim)/dynamic_update_slice | solution.py:202
  81.9 8.2 %dynamic_update_slice.19 = f32[8,128,2,256]{1,0,3,2:T(8,128)} dynamic-update-slice(f32[8,128,2,256]{1,0,3,2:T(8,128)} %get-tuple-element.428, f32[1,128,2,256]{1,0,3,2:T(1,128)S(1)} %copy.336, s32[]{:T(128)} %get-tuple-element.424, s32[]{:T(128)} %constant.38.clone.1..sunk, s32[]{:T(128)} %constant.38.clone.1..sunk, s32[]{:T(128)} %constant.38.clone.1..sunk) | dynamic-update-slice | bytes 524292 | tf_op jit(solution)/shard_map/while/body/jit(dynamic_update_index_in_dim)/dynamic_update_slice | solution.py:202
  94.7 8.2 %dynamic_update_slice.19 = f32[8,128,2,256]{1,0,3,2:T(8,128)} dynamic-update-slice(f32[8,128,2,256]{1,0,3,2:T(8,128)} %get-tuple-element.428, f32[1,128,2,256]{1,0,3,2:T(1,128)S(1)} %copy.336, s32[]{:T(128)} %get-tuple-element.424, s32[]{:T(128)} %constant.38.clone.1..sunk, s32[]{:T(128)} %constant.38.clone.1..sunk, s32[]{:T(128)} %constant.38.clone.1..sunk) | dynamic-update-slice | bytes 524292 | tf_op jit(solution)/shard_map/while/body/jit(dynamic_update_index_in_dim)/dynamic_update_slice | solution.py:202
  107.5 8.2 %dynamic_update_slice.19 = f32[8,128,2,256]{1,0,3,2:T(8,128)} dynamic-update-slice(f32[8,128,2,256]{1,0,3,2:T(8,128)} %get-tuple-element.428, f32[1,128,2,256]{1,0,3,2:T(1,128)S(1)} %copy.336, s32[]{:T(128)} %get-tuple-element.424, s32[]{:T(128)} %constant.38.clone.1..sunk, s32[]{:T(128)} %constant.38.clone.1..sunk, s32[]{:T(128)} %constant.38.clone.1..sunk) | dynamic-update-slice | bytes 524292 | tf_op jit(solution)/shard_map/while/body/jit(dynamic_update_index_in_dim)/dynamic_update_slice | solution.py:202
  117.4 3.0 all-gather.5
  122.3 13.0 %all-gather.6 = bf16[4,516,128]{2,1,0:T(8,128)(2,1)S(1)} all-gather(bf16[1,516,128]{2,1,0:T(8,128)(2,1)S(1)} %maximum_bitcast_fusion.1), channel_id=3, replica_groups=mesh['sp_0'=4,'sp_1'=4,'sp_2'=2,'tp'=4] {'sp_1'}, dimensions={0}, use_global_device_ids=true | all-gather | bytes 660480 | tf_op jit(solution)/shard_map/all_gather | solution.py:28
  136.8 14.1 %all-gather.7 = bf16[4,516,128]{2,1,0:T(8,128)(2,1)S(1)} all-gather(bf16[1,516,128]{2,1,0:T(8,128)(2,1)S(1)} %maximum_bitcast_fusion.2), channel_id=4, replica_groups=mesh['sp_0'=4,'sp_1'=4,'sp_2'=2,'tp'=4] {'sp_0'}, dimensions={0}, use_global_device_ids=true | all-gather | bytes 660480 | tf_op jit(solution)/shard_map/all_gather | solution.py:28
  161.7 14.4 %all_to_all.19 = bf16[4,256,512]{2,1,0:T(8,128)(2,1)S(1)} all-to-all(bf16[4,256,512]{2,1,0:T(8,128)(2,1)S(1)} %bitcast.610), channel_id=1, replica_groups=mesh['sp_0'=4,'sp_1'=4,'sp_2'=2,'tp'=4] {'tp'}, dimensions={0} | all-to-all | bytes 2097152 | tf_op jit(solution)/shard_map/all_to_all | solution.py:249
  176.6 5.7 %fusion.40 = bf16[256,2048]{1,0:T(8,128)(2,1)S(1)} fusion(bf16[256,2048]{0,1:T(8,128)(2,1)S(1)} %bitcast.606, bf16[2048,2048]{1,0:T(8,128)(2,1)} %all-gather.14.cloned.1.call-done, bf16[256,2048]{1,0:T(8,128)(2,1)S(1)} %copy-done), kind=kOutput, calls=%fused_computation.77 | convolution fusion | flops 2149056512 | bytes 11534336 | tf_op jit(solution)/shard_map/dot_general | solution.py:250
  184.1 3.8 copy.246
  188.9 45.1 %all-gather.16.cloned.1.call-done = bf16[1024,2048]{1,0:T(8,128)(2,1)} async-done(((bf16[256,2048]{1,0:T(8,128)(2,1)}), bf16[1024,2048]{1,0:T(8,128)(2,1)}) %all-gather.16.cloned.1.call-update) | async-done | bytes 4194320 | tf_op jit(solution)/shard_map/all_gather | solution.py:259
  234.8 4.0 collective-permute-start
  238.9 16.3 %all-gather.22.cloned.1.call-done = bf16[32,1408,64]{1,0,2:T(8,128)(2,1)} async-done(((bf16[16,1408,64]{1,0,2:T(8,128)(2,1)}), bf16[32,1408,64]{1,0,2:T(8,128)(2,1)}) %all-gather.22.cloned.1.call-update) | async-done | bytes 5767184 | tf_op jit(solution)/shard_map/all_gather | solution.py:85
  255.2 7.0 %copy.200 = bf16[16,2,1408,64]{2,3,1,0:T(8,128)(2,1)} copy(bf16[16,2,1408,64]{2,0,1,3:T(8,128)(2,1)} %bitcast.607) | data formatting | bytes 11534336 | tf_op jit(solution)/shard_map/transpose | solution.py:88
  262.2 56.7 %all-gather.18.cloned.1.call-done = bf16[2048,2816]{1,0:T(8,128)(2,1)} async-done(((bf16[64,2816]{1,0:T(8,128)(2,1)}), bf16[2048,2816]{1,0:T(8,128)(2,1)}) %all-gather.18.cloned.1.call-update) | async-done | bytes 11534352 | tf_op jit(solution)/shard_map/all_gather | solution.py:69
  318.9 11.9 %fusion.37 = f32[1026,1408]{1,0:T(8,128)} fusion(bf16[2048,2816]{1,0:T(8,128)(2,1)} %all-gather.18.cloned.1.call-done, bf16[1024,2048]{1,0:T(8,128)(2,1)} %all-gather.16.cloned.1.call-done, bf16[2,2048]{1,0:T(2,128)(2,1)S(1)} %collective-permute-done), kind=kOutput, calls=%fused_computation.69 | convolution fusion | flops 5925519360 | bytes 15748096 | tf_op jit(solution)/shard_map/dot_general | solution.py:263
  330.9 8.7 %fusion.33 = f32[1026,1408]{1,0:T(8,128)} fusion(bf16[2048,2816]{1,0:T(8,128)(2,1)S(1)} %copy-done.13, bf16[1024,2048]{1,0:T(8,128)(2,1)S(1)} %copy-done.12, bf16[2,2048]{1,0:T(2,128)(2,1)S(1)} %collective-permute-done), kind=kOutput, calls=%fused_computation.62 | convolution fusion | flops 5925519360 | bytes 15748096 | tf_op jit(solution)/shard_map/dot_general | solution.py:264
  339.5 24.1 %convolution_convert_fusion = bf16[1024,2048]{1,0:T(8,128)(2,1)} fusion(bf16[1408,2048]{0,1:T(8,128)(2,1)} %bitcast.608, f32[1026,1408]{1,0:T(8,128)} %fusion.33, f32[1026,1408]{1,0:T(8,128)} %fusion.37, f32[1408]{0:T(1024)S(1)} %get-tuple-element.181, f32[1408]{0:T(1024)S(1)} %get-tuple-element.182, f32[1408]{0:T(1024)S(1)} %get-tuple-element.180, ...), kind=kOutput, calls=%fused_computation.72 | convolution fusion | flops 5930745856 | bytes 44598272 | tf_op jit(solution)/shard_map/dot_general | solution.py:278
  363.7 46.0 %reduce-scatter.2.cloned.1.call-done = bf16[256,2048]{1,0:T(8,128)(2,1)} async-done(((bf16[1024,2048]{1,0:T(8,128)(2,1)}), bf16[256,2048]{1,0:T(8,128)(2,1)}) %reduce-scatter.2.cloned.1.call-update) | async-done | bytes 1048592 | tf_op jit(solution)/shard_map/reduce_scatter | solution.py:277
  (365 shorter events, 64.2 us)
Async XLA Ops:
  6.5 3.9 copy-start.10
  6.5 4.2 copy-start.1
  6.5 170.0 %all-gather.14.cloned.1.call-start = ((), (), s32[]{:S(2)}) async-start(), calls=%async_computation.2 | async-start | bytes 10485760 | tf_op jit(solution)/shard_map/all_gather | solution.py:248
  7.3 176.8 %all-gather.20.cloned.1.call-start = ((), (), s32[]{:S(2)}) async-start(), calls=%async_computation.6 | async-start | bytes 3063808 | tf_op jit(solution)/shard_map/all_gather | solution.py:85
  8.0 226.0 %all-gather.16.cloned.1.call-start = ((), (), s32[]{:S(2)}) async-start(), calls=%async_computation.3 | async-start | bytes 5242880 | tf_op jit(solution)/shard_map/all_gather | solution.py:259
  116.1 34.9 %copy-start.4 = (f32[8,128,2]{2,1,0:T(8,128)S(1)}, f32[8,128,2]{2,1,0:T(8,128)}, u32[]{:S(2)}) copy-start(f32[8,128,2]{2,1,0:T(8,128)} %get-tuple-element.72) | copy-start | bytes 24580
  116.1 35.1 %copy-start.3 = (f32[8,128,2]{2,1,0:T(8,128)S(1)}, f32[8,128,2]{2,1,0:T(8,128)}, u32[]{:S(2)}) copy-start(f32[8,128,2]{2,1,0:T(8,128)} %get-tuple-element.77) | copy-start | bytes 24580
  153.1 2.6 copy-start.2
  155.7 1.3 copy-start.11
  159.2 17.4 %copy-start = (bf16[256,2048]{1,0:T(8,128)(2,1)S(1)}, bf16[256,2048]{1,0:T(8,128)(2,1)}, u32[]{:S(2)}) copy-start(bf16[256,2048]{1,0:T(8,128)(2,1)} %param.18) | copy-start | bytes 3145732
  176.6 6.0 %copy-start.9 = (f32[2048]{0:T(1024)S(1)}, f32[2048]{0:T(1024)}, u32[]{:S(2)}) copy-start(f32[2048]{0:T(1024)} %param.28) | copy-start | bytes 24580
  184.0 71.2 %all-gather.22.cloned.1.call-start = ((), (), s32[]{:S(2)}) async-start(), calls=%async_computation.7 | async-start | bytes 8650752 | tf_op jit(solution)/shard_map/all_gather | solution.py:85
  184.0 4.0 copy-start.5
  184.0 4.0 copy-start.6
  184.1 54.8 %copy-start.7 = (f32[3,1408]{1,0:T(4,128)S(1)}, f32[3,1408]{1,0:T(4,128)}, u32[]{:S(2)}) copy-start(f32[3,1408]{1,0:T(4,128)} %param.32) | copy-start | bytes 50692
  184.1 54.8 %copy-start.8 = (f32[3,1408]{1,0:T(4,128)S(1)}, f32[3,1408]{1,0:T(4,128)}, u32[]{:S(2)}) copy-start(f32[3,1408]{1,0:T(4,128)} %param.31) | copy-start | bytes 50692
  187.9 131.0 %all-gather.18.cloned.1.call-start = ((), (), s32[]{:S(2)}) async-start(), calls=%async_computation.4 | async-start | bytes 11894784 | tf_op jit(solution)/shard_map/all_gather | solution.py:69
  188.8 220.8 %reduce-scatter.2.cloned.1.call-start = ((), (), s32[]{:S(2)}) async-start(), calls=%async_computation.5 | async-start | bytes 5242880 | tf_op jit(solution)/shard_map/reduce_scatter | solution.py:277
  234.8 27.4 %collective-permute-start = (bf16[2,2048]{1,0:T(2,128)(2,1)S(1)}, bf16[2,2048]{1,0:T(2,128)(2,1)S(1)}, u32[]{:S(2)}, u32[]{:S(2)}) collective-permute-start(bf16[2,2048]{1,0:T(2,128)(2,1)S(1)} %slice.352), channel_id=1, source_target_pairs={{0,4},{4,8},{8,12},{12,16},{16,20},{20,24},{24,28},{28,32},{32,36}... | collective-permute-start | bytes 24584 | tf_op jit(solution)/shard_map/ppermute | solution.py:64
  318.9 11.9 %copy-start.12 = (bf16[1024,2048]{1,0:T(8,128)(2,1)S(1)}, bf16[1024,2048]{1,0:T(8,128)(2,1)}, u32[]{:S(2)}) copy-start(bf16[1024,2048]{1,0:T(8,128)(2,1)} %all-gather.16.cloned.1.call-done) | copy-start | bytes 12582916
  318.9 11.9 %copy-start.13 = (bf16[2048,2816]{1,0:T(8,128)(2,1)S(1)}, bf16[2048,2816]{1,0:T(8,128)(2,1)}, u32[]{:S(2)}) copy-start(bf16[2048,2816]{1,0:T(8,128)(2,1)} %all-gather.18.cloned.1.call-done) | copy-start | bytes 34603012
Sparse Core Ops, SparseCore 0:
  9.0 86.0 all-gather.13
  97.3 51.0 all-gather.19
  184.1 49.8 all-gather.15
  235.5 19.6 all-gather.21
  257.3 61.5 all-gather.17
  363.8 45.7 reduce-scatter.1
where the time goes:
time: 421 us; the launch traced here: 419 us
  waiting for transfers between devices  166 us (39%)
  local copies, waits for them, and re-layouts  105 us (25%)
  matrix products  62 us (15%)
  blocking collectives  44.6 us (11%)
  other arithmetic  23.2 us (6%)
  between operations  14.1 us (3%)
  starting transfers between devices  4.22 us (1%)
    dynamic_update_slice x16, local copies, waits for them, and re-layouts, local(): lax.scan(local_step, initial, (blocks(queries_low), blocks(keys_low), blo...  66.9 us
    all_gather x1, waiting for transfers between devices, side_by_side(): lax.all_gather(both, axis, axis=dim, tiled=True)  56.7 us
    reduce_scatter x1, waiting for transfers between devices, local(): lax.psum_scatter(jnp.dot(hidden, whole_down, preferred_element_type=jnp.f...  46 us
    all_gather x1, waiting for transfers between devices, local(): group_rows = lax.all_gather(normed_rows, 'tp', axis=0, tiled=True)  45.1 us
    all_gather x3, blocking collectives, gathered_once(): both, at, found = (lax.all_gather(jnp.concatenate(lines), axis), 0, {})  30.2 us
    dot_general x1, matrix products, local(): jnp.dot(hidden, whole_down, preferred_element_type=jnp.float32)  24.1 us
    all_gather x2, waiting for transfers between devices, all_blocks(): tiles = lax.all_gather(tiles, axes[k])  16.3 us
    all_to_all x1, blocking collectives, local(): lax.all_to_all(gated_rows, 'tp', split_axis=0, concat_axis=1, tiled=True)  14.4 us
  transfers between devices with their start and end apart: 7, of which 4 were waited for; matrix products, arithmetic and copies ran while one was open for 34% of the time, Pallas kernels for 0%

commit v1 on v0

--- a/solution.py
+++ b/solution.py
@@ -256,7 +256,12 @@
         * lax.rsqrt(jnp.mean(stream_wide * stream_wide, axis=-1, keepdims=True) + eps)
         * feedforward_norm_gain[None, :]
     ).astype(jnp.bfloat16)
-    group_rows = lax.all_gather(normed_rows, "tp", axis=0, tiled=True)
+    ring = [normed_rows]
+    for hop in range(3):
+        ring.append(lax.ppermute(ring[-1], "tp", [(dev, (dev + 1) % 4) for dev in range(4)]))
+    group_rows = jnp.roll(
+        jnp.concatenate(ring[::-1], axis=0), (lax.axis_index("tp") + 1) * ring[0].shape[0], axis=0
+    )
     earlier_rows = shifted(group_rows[-2:], SP, 1)
     window = jnp.concatenate([earlier_rows, group_rows], axis=0)
     pieces = side_by_side((gate_up_weight, value_up_weight), SP, 0, 1)

time: 421 us -> 419 us (level)
  waiting for transfers between devices: 166 us -> 151 us
  starting transfers between devices: 4.22 us -> 13.5 us
  local copies, waits for them, and re-layouts: 105 us -> 112 us
  blocking collectives: 44.6 us -> 40 us
    all_gather x1, waiting for transfers between devices: 56.7 us -> 0.01 us  [side_by_side(): lax.all_gather(both, axis, axis=dim, tiled=True)]
    ppermute x0 -> x3, waiting for transfers between devices: none -> 54.1 us  [local(): lax.ppermute(ring[-1], 'tp', [(dev, (dev + 1) % 4) for dev in range(4)])]
    all_gather x1 -> x0, waiting for transfers between devices: 45.1 us -> none  [local(): group_rows = lax.all_gather(normed_rows, 'tp', axis=0, tiled=True)]
    all_gather x2, waiting for transfers between devices: 16.3 us -> 51.1 us  [all_blocks(): tiles = lax.all_gather(tiles, axes[k])]
    ppermute x1, starting transfers between devices: 4.02 us -> 12.7 us  [shifted(): return lax.ppermute(x, axis, pairs)]
    all_gather x3, blocking collectives: 30.2 us -> 25.8 us  [gathered_once(): both, at, found = (lax.all_gather(jnp.concatenate(lines), axis), 0, {})]
  transfers between devices with their start and end apart: 7 -> 9, of which waited for: 4 -> 5; matrix products, arithmetic and copies ran while one was open for 34% -> 36% of each run, Pallas kernels for 0% -> 0%
where the time goes in v1:
time: 419 us; the launch traced here: 417 us
  waiting for transfers between devices  151 us (36%)
  local copies, waits for them, and re-layouts  112 us (27%)
  matrix products  63.1 us (15%)
  blocking collectives  40 us (10%)
  other arithmetic  22 us (5%)
  between operations  13.7 us (3%)
  starting transfers between devices  13.5 us (3%)
    dynamic_update_slice x16, local copies, waits for them, and re-layouts, local(): lax.scan(local_step, initial, (blocks(queries_low), blocks(keys_low), blo...  66.7 us
    ppermute x3, waiting for transfers between devices, local(): lax.ppermute(ring[-1], 'tp', [(dev, (dev + 1) % 4) for dev in range(4)])  54.1 us
    all_gather x2, waiting for transfers between devices, all_blocks(): tiles = lax.all_gather(tiles, axes[k])  51.1 us
    reduce_scatter x1, waiting for transfers between devices, local(): lax.psum_scatter(jnp.dot(hidden, whole_down, preferred_element_type=jnp.f...  44.7 us
    all_gather x3, blocking collectives, gathered_once(): both, at, found = (lax.all_gather(jnp.concatenate(lines), axis), 0, {})  25.8 us
    dot_general x1, matrix products, local(): jnp.dot(hidden, whole_down, preferred_element_type=jnp.float32)  24.2 us
    all_to_all x1, blocking collectives, local(): lax.all_to_all(gated_rows, 'tp', split_axis=0, concat_axis=1, tiled=True)  14.2 us
    ppermute x1, starting transfers between devices, shifted(): return lax.ppermute(x, axis, pairs)  12.7 us
  transfers between devices with their start and end apart: 9, of which 5 were waited for; matrix products, arithmetic and copies ran while one was open for 36% of the time, Pallas kernels for 0%

profile of v1, /device:TPU:1, one launch (start us, length us, event | category | flops | bytes accessed | tf_op | source)
XLA Modules:
  0.0 416.8 jit_solution(6871465984757861809)
XLA Ops:
  8.1 51.1 %all-gather.17.cloned.1.call-done = bf16[22528,64]{0,1:T(8,128)(2,1)} async-done(((bf16[1408,64]{0,1:T(8,128)(2,1)}), bf16[22528,64]{0,1:T(8,128)(2,1)}) %all-gather.17.cloned.1.call-update) | async-done | bytes 2883600 | tf_op jit(solution)/shard_map/all_gather | solution.py:85
  59.2 3.9 copy.246
  68.8 102.3 %while.21 = (s32[]{:T(128)}, f32[2,256,128]{2,1,0:T(8,128)S(1)}, f32[2,128]{1,0:T(2,128)S(1)}, f32[2]{0:T(128)S(1)}, f32[8,128,2,256]{1,0,3,2:T(8,128)}, /*index...) while((s32[]{:T(128)}, f32[2,256,128]{2,1,0:T(8,128)S(1)}, ...), condition=%wide.region_6.7_spmd.clone, body=%wide.region_0.6_spmd.clone.sunk | while | flops 59952648 | bytes 4685610 | solution.py:202
  73.0 8.2 %dynamic_update_slice.19 = f32[8,128,2,256]{1,0,3,2:T(8,128)} dynamic-update-slice(f32[8,128,2,256]{1,0,3,2:T(8,128)} %get-tuple-element.428, f32[1,128,2,256]{1,0,3,2:T(1,128)S(1)} %copy.336, s32[]{:T(128)} %get-tuple-element.424, s32[]{:T(128)} %constant.93.clone.1..sunk, s32[]{:T(128)} %constant.93.clone.1..sunk, s32[]{:T(128)} %constant.93.clone.1..sunk) | dynamic-update-slice | bytes 524292 | tf_op jit(solution)/shard_map/while/body/jit(dynamic_update_index_in_dim)/dynamic_update_slice | solution.py:202
  85.8 8.2 %dynamic_update_slice.19 = f32[8,128,2,256]{1,0,3,2:T(8,128)} dynamic-update-slice(f32[8,128,2,256]{1,0,3,2:T(8,128)} %get-tuple-element.428, f32[1,128,2,256]{1,0,3,2:T(1,128)S(1)} %copy.336, s32[]{:T(128)} %get-tuple-element.424, s32[]{:T(128)} %constant.93.clone.1..sunk, s32[]{:T(128)} %constant.93.clone.1..sunk, s32[]{:T(128)} %constant.93.clone.1..sunk) | dynamic-update-slice | bytes 524292 | tf_op jit(solution)/shard_map/while/body/jit(dynamic_update_index_in_dim)/dynamic_update_slice | solution.py:202
  98.6 8.2 %dynamic_update_slice.19 = f32[8,128,2,256]{1,0,3,2:T(8,128)} dynamic-update-slice(f32[8,128,2,256]{1,0,3,2:T(8,128)} %get-tuple-element.428, f32[1,128,2,256]{1,0,3,2:T(1,128)S(1)} %copy.336, s32[]{:T(128)} %get-tuple-element.424, s32[]{:T(128)} %constant.93.clone.1..sunk, s32[]{:T(128)} %constant.93.clone.1..sunk, s32[]{:T(128)} %constant.93.clone.1..sunk) | dynamic-update-slice | bytes 524292 | tf_op jit(solution)/shard_map/while/body/jit(dynamic_update_index_in_dim)/dynamic_update_slice | solution.py:202
  111.4 8.2 %dynamic_update_slice.19 = f32[8,128,2,256]{1,0,3,2:T(8,128)} dynamic-update-slice(f32[8,128,2,256]{1,0,3,2:T(8,128)} %get-tuple-element.428, f32[1,128,2,256]{1,0,3,2:T(1,128)S(1)} %copy.336, s32[]{:T(128)} %get-tuple-element.424, s32[]{:T(128)} %constant.93.clone.1..sunk, s32[]{:T(128)} %constant.93.clone.1..sunk, s32[]{:T(128)} %constant.93.clone.1..sunk) | dynamic-update-slice | bytes 524292 | tf_op jit(solution)/shard_map/while/body/jit(dynamic_update_index_in_dim)/dynamic_update_slice | solution.py:202
  124.2 8.2 %dynamic_update_slice.19 = f32[8,128,2,256]{1,0,3,2:T(8,128)} dynamic-update-slice(f32[8,128,2,256]{1,0,3,2:T(8,128)} %get-tuple-element.428, f32[1,128,2,256]{1,0,3,2:T(1,128)S(1)} %copy.336, s32[]{:T(128)} %get-tuple-element.424, s32[]{:T(128)} %constant.93.clone.1..sunk, s32[]{:T(128)} %constant.93.clone.1..sunk, s32[]{:T(128)} %constant.93.clone.1..sunk) | dynamic-update-slice | bytes 524292 | tf_op jit(solution)/shard_map/while/body/jit(dynamic_update_index_in_dim)/dynamic_update_slice | solution.py:202
  137.0 8.2 %dynamic_update_slice.19 = f32[8,128,2,256]{1,0,3,2:T(8,128)} dynamic-update-slice(f32[8,128,2,256]{1,0,3,2:T(8,128)} %get-tuple-element.428, f32[1,128,2,256]{1,0,3,2:T(1,128)S(1)} %copy.336, s32[]{:T(128)} %get-tuple-element.424, s32[]{:T(128)} %constant.93.clone.1..sunk, s32[]{:T(128)} %constant.93.clone.1..sunk, s32[]{:T(128)} %constant.93.clone.1..sunk) | dynamic-update-slice | bytes 524292 | tf_op jit(solution)/shard_map/while/body/jit(dynamic_update_index_in_dim)/dynamic_update_slice | solution.py:202
  149.7 8.2 %dynamic_update_slice.19 = f32[8,128,2,256]{1,0,3,2:T(8,128)} dynamic-update-slice(f32[8,128,2,256]{1,0,3,2:T(8,128)} %get-tuple-element.428, f32[1,128,2,256]{1,0,3,2:T(1,128)S(1)} %copy.336, s32[]{:T(128)} %get-tuple-element.424, s32[]{:T(128)} %constant.93.clone.1..sunk, s32[]{:T(128)} %constant.93.clone.1..sunk, s32[]{:T(128)} %constant.93.clone.1..sunk) | dynamic-update-slice | bytes 524292 | tf_op jit(solution)/shard_map/while/body/jit(dynamic_update_index_in_dim)/dynamic_update_slice | solution.py:202
  162.6 8.2 %dynamic_update_slice.19 = f32[8,128,2,256]{1,0,3,2:T(8,128)} dynamic-update-slice(f32[8,128,2,256]{1,0,3,2:T(8,128)} %get-tuple-element.428, f32[1,128,2,256]{1,0,3,2:T(1,128)S(1)} %copy.336, s32[]{:T(128)} %get-tuple-element.424, s32[]{:T(128)} %constant.93.clone.1..sunk, s32[]{:T(128)} %constant.93.clone.1..sunk, s32[]{:T(128)} %constant.93.clone.1..sunk) | dynamic-update-slice | bytes 524292 | tf_op jit(solution)/shard_map/while/body/jit(dynamic_update_index_in_dim)/dynamic_update_slice | solution.py:202
  177.2 12.4 %all-gather.6 = bf16[4,516,128]{2,1,0:T(8,128)(2,1)S(1)} all-gather(bf16[1,516,128]{2,1,0:T(8,128)(2,1)S(1)} %maximum_bitcast_fusion.1), channel_id=3, replica_groups=mesh['sp_0'=4,'sp_1'=4,'sp_2'=2,'tp'=4] {'sp_1'}, dimensions={0}, use_global_device_ids=true | all-gather | bytes 660480 | tf_op jit(solution)/shard_map/all_gather | solution.py:28
  191.0 10.5 %all-gather.7 = bf16[4,516,128]{2,1,0:T(8,128)(2,1)S(1)} all-gather(bf16[1,516,128]{2,1,0:T(8,128)(2,1)S(1)} %maximum_bitcast_fusion.2), channel_id=4, replica_groups=mesh['sp_0'=4,'sp_1'=4,'sp_2'=2,'tp'=4] {'sp_0'}, dimensions={0}, use_global_device_ids=true | all-gather | bytes 660480 | tf_op jit(solution)/shard_map/all_gather | solution.py:28
  215.5 14.2 %all_to_all.19 = bf16[4,256,512]{2,1,0:T(8,128)(2,1)S(1)} all-to-all(bf16[4,256,512]{2,1,0:T(8,128)(2,1)S(1)} %bitcast.610), channel_id=1, replica_groups=mesh['sp_0'=4,'sp_1'=4,'sp_2'=2,'tp'=4] {'tp'}, dimensions={0} | all-to-all | bytes 2097152 | tf_op jit(solution)/shard_map/all_to_all | solution.py:249
  230.3 5.7 %fusion.40 = bf16[256,2048]{1,0:T(8,128)(2,1)S(1)} fusion(bf16[256,2048]{0,1:T(8,128)(2,1)S(1)} %bitcast.606, bf16[2048,2048]{1,0:T(8,128)(2,1)} %all-gather.13.cloned.1.call-done, bf16[256,2048]{1,0:T(8,128)(2,1)S(1)} %copy-done.1), kind=kOutput, calls=%fused_computation.77 | convolution fusion | flops 2149056512 | bytes 11534336 | tf_op jit(solution)/shard_map/dot_general | solution.py:250
  237.3 18.0 %collective-permute-done = bf16[256,2048]{1,0:T(8,128)(2,1)S(1)} collective-permute-done((bf16[256,2048]{1,0:T(8,128)(2,1)S(1)}, bf16[256,2048]{1,0:T(8,128)(2,1)S(1)}, u32[]{:S(2)}, u32[]{:S(2)}) %collective-permute-start) | collective-permute-done | bytes 1048608 | tf_op jit(solution)/shard_map/ppermute | solution.py:261
  255.3 21.6 %collective-permute-done.1 = bf16[256,2048]{1,0:T(8,128)(2,1)S(1)} collective-permute-done((bf16[256,2048]{1,0:T(8,128)(2,1)S(1)}, bf16[256,2048]{1,0:T(8,128)(2,1)S(1)}, u32[]{:S(2)}, u32[]{:S(2)}) %collective-permute-start.1) | collective-permute-done | bytes 1048608 | tf_op jit(solution)/shard_map/ppermute | solution.py:261
  277.0 7.1 %copy.200 = bf16[16,2,1408,64]{2,3,1,0:T(8,128)(2,1)} copy(bf16[16,2,1408,64]{2,0,1,3:T(8,128)(2,1)} %bitcast.607) | data formatting | bytes 11534336 | tf_op jit(solution)/shard_map/transpose | solution.py:88
  284.1 14.5 %collective-permute-done.2 = bf16[256,2048]{1,0:T(8,128)(2,1)} collective-permute-done((bf16[256,2048]{1,0:T(8,128)(2,1)S(1)}, bf16[256,2048]{1,0:T(8,128)(2,1)}, u32[]{:S(2)}, u32[]{:S(2)}) %collective-permute-start.2) | collective-permute-done | bytes 1048608 | tf_op jit(solution)/shard_map/ppermute | solution.py:261
  302.2 12.7 %collective-permute-start.3 = (bf16[2,2048]{1,0:T(2,128)(2,1)S(1)}, bf16[2,2048]{1,0:T(2,128)(2,1)S(1)}, u32[]{:S(2)}, u32[]{:S(2)}) collective-permute-start(bf16[2,2048]{1,0:T(2,128)(2,1)S(1)} %constant_dynamic-slice_fusion.3), channel_id=1, source_target_pairs={{0,4},{4,8},{8,12},{12,16},{16,20},{20,24},{24,28},{28,32},{32,36}... | collective-permute-start | bytes 24584 | tf_op jit(solution)/shard_map/ppermute | solution.py:64
  318.1 12.0 %fusion.37 = f32[1026,1408]{1,0:T(8,128)} fusion(bf16[2048,2816]{1,0:T(8,128)(2,1)} %all-gather.15.cloned.1.call-done, bf16[1024,2048]{1,0:T(8,128)(2,1)} %constant_dynamic-slice_fusion.4, bf16[2,2048]{1,0:T(2,128)(2,1)S(1)} %collective-permute-done.3), kind=kOutput, calls=%fused_computation.69 | convolution fusion | flops 5925519360 | bytes 15748096 | tf_op jit(solution)/shard_map/dot_general | solution.py:268
  330.1 8.7 %fusion.33 = f32[1026,1408]{1,0:T(8,128)} fusion(bf16[2048,2816]{1,0:T(8,128)(2,1)S(1)} %copy-done.12, bf16[1024,2048]{1,0:T(8,128)(2,1)S(1)} %copy-done, bf16[2,2048]{1,0:T(2,128)(2,1)S(1)} %collective-permute-done.3), kind=kOutput, calls=%fused_computation.62 | convolution fusion | flops 5925519360 | bytes 15748096 | tf_op jit(solution)/shard_map/dot_general | solution.py:269
  338.8 24.2 %convolution_convert_fusion = bf16[1024,2048]{1,0:T(8,128)(2,1)} fusion(bf16[1408,2048]{0,1:T(8,128)(2,1)} %bitcast.608, f32[1026,1408]{1,0:T(8,128)} %fusion.33, f32[1026,1408]{1,0:T(8,128)} %fusion.37, f32[1408]{0:T(1024)S(1)} %get-tuple-element.181, f32[1408]{0:T(1024)S(1)} %get-tuple-element.182, f32[1408]{0:T(1024)S(1)} %get-tuple-element.180, ...), kind=kOutput, calls=%fused_computation.72 | convolution fusion | flops 5930745856 | bytes 44598272 | tf_op jit(solution)/shard_map/dot_general | solution.py:283
  363.0 44.7 %reduce-scatter.2.cloned.1.call-done = bf16[256,2048]{1,0:T(8,128)(2,1)} async-done(((bf16[1024,2048]{1,0:T(8,128)(2,1)}), bf16[256,2048]{1,0:T(8,128)(2,1)}) %reduce-scatter.2.cloned.1.call-update) | async-done | bytes 1048592 | tf_op jit(solution)/shard_map/reduce_scatter | solution.py:282
  (375 shorter events, 75.2 us)
Async XLA Ops:
  6.5 56.6 %copy-start.4 = (bf16[64,1408]{1,0:T(8,128)(2,1)S(1)}, bf16[64,1408]{1,0:T(8,128)(2,1)}, u32[]{:S(2)}) copy-start(bf16[64,1408]{1,0:T(8,128)(2,1)} %param.29) | copy-start | bytes 540676
  6.5 56.6 %copy-start.3 = (bf16[64,1408]{1,0:T(8,128)(2,1)S(1)}, bf16[64,1408]{1,0:T(8,128)(2,1)}, u32[]{:S(2)}) copy-start(bf16[64,1408]{1,0:T(8,128)(2,1)} %param.30) | copy-start | bytes 540676
  6.5 52.6 %all-gather.17.cloned.1.call-start = ((), (), s32[]{:S(2)}) async-start(), calls=%async_computation.5 | async-start | bytes 3063808 | tf_op jit(solution)/shard_map/all_gather | solution.py:85
  7.3 56.8 %copy-start.8 = (f32[1024,2]{0,1:T(2,128)S(1)}, f32[1024,2]{0,1:T(2,128)}, u32[]{:S(2)}) copy-start(f32[1024,2]{0,1:T(2,128)} %param.25) | copy-start | bytes 24580
  7.3 56.8 %copy-start.9 = (f32[1024,2]{0,1:T(2,128)S(1)}, f32[1024,2]{0,1:T(2,128)}, u32[]{:S(2)}) copy-start(f32[1024,2]{0,1:T(2,128)} %param.24) | copy-start | bytes 24580
  7.3 223.0 %all-gather.13.cloned.1.call-start = ((), (), s32[]{:S(2)}) async-start(), calls=%async_computation.2 | async-start | bytes 10485760 | tf_op jit(solution)/shard_map/all_gather | solution.py:248
  8.0 269.0 %all-gather.19.cloned.1.call-start = ((), (), s32[]{:S(2)}) async-start(), calls=%async_computation.6 | async-start | bytes 8650752 | tf_op jit(solution)/shard_map/all_gather | solution.py:85
  59.2 6.5 %copy-start.10 = (f32[1024,2]{0,1:T(2,128)S(1)}, f32[1024,2]{0,1:T(2,128)}, u32[]{:S(2)}) copy-start(f32[1024,2]{0,1:T(2,128)} %param.23) | copy-start | bytes 24580
  59.2 6.8 %copy-start.2 = (bf16[1024,256]{1,0:T(8,128)(2,1)S(1)}, bf16[1024,256]{1,0:T(8,128)(2,1)}, u32[]{:S(2)}) copy-start(bf16[1024,256]{1,0:T(8,128)(2,1)} %param.20) | copy-start | bytes 1572868
  63.0 255.1 %all-gather.15.cloned.1.call-start = ((), (), s32[]{:S(2)}) async-start(), calls=%async_computation.3 | async-start | bytes 11894784 | tf_op jit(solution)/shard_map/all_gather | solution.py:69
  63.9 343.8 %reduce-scatter.2.cloned.1.call-start = ((), (), s32[]{:S(2)}) async-start(), calls=%async_computation.4 | async-start | bytes 5242880 | tf_op jit(solution)/shard_map/reduce_scatter | solution.py:282
  208.4 2.3 copy-start.11
  210.9 19.3 %copy-start.1 = (bf16[256,2048]{1,0:T(8,128)(2,1)S(1)}, bf16[256,2048]{1,0:T(8,128)(2,1)}, u32[]{:S(2)}) copy-start(bf16[256,2048]{1,0:T(8,128)(2,1)} %param.18) | copy-start | bytes 3145732
  230.3 6.1 %copy-start.5 = (f32[2048]{0:T(1024)S(1)}, f32[2048]{0:T(1024)}, u32[]{:S(2)}) copy-start(f32[2048]{0:T(1024)} %param.28) | copy-start | bytes 24580
  230.3 46.6 %copy-start.6 = (f32[3,1408]{1,0:T(4,128)S(1)}, f32[3,1408]{1,0:T(4,128)}, u32[]{:S(2)}) copy-start(f32[3,1408]{1,0:T(4,128)} %param.32) | copy-start | bytes 50692
  230.3 46.6 %copy-start.7 = (f32[3,1408]{1,0:T(4,128)S(1)}, f32[3,1408]{1,0:T(4,128)}, u32[]{:S(2)}) copy-start(f32[3,1408]{1,0:T(4,128)} %param.31) | copy-start | bytes 50692
  236.7 18.6 %collective-permute-start = (bf16[256,2048]{1,0:T(8,128)(2,1)S(1)}, bf16[256,2048]{1,0:T(8,128)(2,1)S(1)}, u32[]{:S(2)}, u32[]{:S(2)}) collective-permute-start(bf16[256,2048]{1,0:T(8,128)(2,1)S(1)} %fusion.43), channel_id=1, source_target_pairs={{0,1},{1,2},{2,3},{3,0},{4,5},{5,6},{6,7},{7,4},{8,9},{9,10},{10,1... | collective-permute-start | bytes 3145736 | tf_op jit(solution)/shard_map/ppermute | solution.py:261
  255.3 21.6 %collective-permute-start.1 = (bf16[256,2048]{1,0:T(8,128)(2,1)S(1)}, bf16[256,2048]{1,0:T(8,128)(2,1)S(1)}, u32[]{:S(2)}, u32[]{:S(2)}) collective-permute-start(bf16[256,2048]{1,0:T(8,128)(2,1)S(1)} %collective-permute-done), channel_id=1, source_target_pairs={{0,1},{1,2},{2,3},{3,0},{4,5},{5,6},{6,7},{7,4},{8,9},{9,10},{10,1... | collective-permute-start | bytes 3145736 | tf_op jit(solution)/shard_map/ppermute | solution.py:261
  276.9 21.7 %collective-permute-start.2 = (bf16[256,2048]{1,0:T(8,128)(2,1)S(1)}, bf16[256,2048]{1,0:T(8,128)(2,1)}, u32[]{:S(2)}, u32[]{:S(2)}) collective-permute-start(bf16[256,2048]{1,0:T(8,128)(2,1)S(1)} %collective-permute-done.1), channel_id=1, source_target_pairs={{0,1},{1,2},{2,3},{3,0},{4,5},{5,6},{6,7},{7,4},{8,9},{9,10},{10,1... | collective-permute-start | bytes 3145736 | tf_op jit(solution)/shard_map/ppermute | solution.py:261
  302.2 15.9 %collective-permute-start.3 = (bf16[2,2048]{1,0:T(2,128)(2,1)S(1)}, bf16[2,2048]{1,0:T(2,128)(2,1)S(1)}, u32[]{:S(2)}, u32[]{:S(2)}) collective-permute-start(bf16[2,2048]{1,0:T(2,128)(2,1)S(1)} %constant_dynamic-slice_fusion.3), channel_id=1, source_target_pairs={{0,4},{4,8},{8,12},{12,16},{16,20},{20,24},{24,28},{28,32},{32,36}... | collective-permute-start | bytes 24584 | tf_op jit(solution)/shard_map/ppermute | solution.py:64
  318.1 12.0 %copy-start = (bf16[1024,2048]{1,0:T(8,128)(2,1)S(1)}, bf16[1024,2048]{1,0:T(8,128)(2,1)}, u32[]{:S(2)}) copy-start(bf16[1024,2048]{1,0:T(8,128)(2,1)} %constant_dynamic-slice_fusion.4) | copy-start | bytes 12582916
  318.1 12.0 %copy-start.12 = (bf16[2048,2816]{1,0:T(8,128)(2,1)S(1)}, bf16[2048,2816]{1,0:T(8,128)(2,1)}, u32[]{:S(2)}) copy-start(bf16[2048,2816]{1,0:T(8,128)(2,1)} %all-gather.15.cloned.1.call-done) | copy-start | bytes 34603012
Sparse Core Ops, SparseCore 0:
  9.5 49.5 all-gather.16
  60.8 82.4 all-gather.12
  145.0 20.2 all-gather.18
  167.4 63.4 all-gather.14
  363.1 44.5 reduce-scatter.1
